TPU v7x, 32 devices: a whole 2x2x4 slice. The times are simulated.
32 devices in a mesh: ep: 8 (over z, x), tp: 4 (over y, core).
Axes of the slice: x: 2, y: 2, z: 4, core: 2. Of those that a mesh axis runs over, the one named last changes fastest.
Arguments:
- hidden_in: bfloat16 [128, 1024], P('ep'), may hold values from -6 to 6
- attn_gain: float32 [1024], replicated, may hold values from 0.1 to 1.9
- w_qdown: bfloat16 [1024, 256], replicated, may hold values from -0.1875 to 0.1875
- q_gain: float32 [256], replicated, may hold values from 0.1 to 1.9
- w_qnope: bfloat16 [256, 512], replicated, may hold values from -0.375 to 0.375
- w_qrope: bfloat16 [256, 256], replicated, may hold values from -0.375 to 0.375
- w_kvdown: bfloat16 [1024, 128], replicated, may hold values from -0.1875 to 0.1875
- kv_gain: float32 [128], replicated, may hold values from 0.1 to 1.9
- w_krope: bfloat16 [1024, 32], replicated, may hold values from -0.1875 to 0.1875
- w_ukey: bfloat16 [128, 512], replicated, may hold values from -0.75 to 0.75
- w_uvalue: bfloat16 [128, 512], replicated, may hold values from -0.5 to 0.5
- w_out: bfloat16 [512, 1024], P('tp'), may hold values from -0.25 to 0.25
- cache_latent: bfloat16 [128, 1024, 128], P(('ep', 'tp')), may hold values from -6 to 6
- cache_rope: bfloat16 [128, 32, 1024], P(('ep', 'tp')), may hold values from -900 to 900
- lengths: int32 [128], P(('ep', 'tp')), may hold values from 1 to 1024, as said below
- ffn_gain: float32 [1024], replicated, may hold values from 0.1 to 1.9
- routes: int32 [128, 2], P('ep'), may hold values from 0 to 3, all different within a row; in each aligned block of 16 rows (0 to 15, 16 to 31, ...) at most 16 rows name the same one
- route_weights: float32 [128, 2], P('ep'), may hold values from 0.25 to 1
- w_gate: bfloat16 [8, 1024, 1792], P('ep', None, 'tp'), may hold values from -0.1875 to 0.1875
- w_up: bfloat16 [8, 1024, 1792], P('ep', None, 'tp'), may hold values from -0.1875 to 0.1875
- w_down: bfloat16 [8, 1792, 1024], P('ep', 'tp'), may hold values from -0.09375 to 0.09375
Outputs:
- next_hidden: bfloat16 [128, 1024], P('ep', 'tp')
Inputs may be any that keep to these rules, and one draw needn't show every extreme that they name: `lengths`: each sequence has 1 to 1024 valid cached positions; in every aligned block of 16 sequences one has all 1024. `routes`: each row names two different experts. In the aligned blocks of 16 rows no expert is named by more than 16 rows, and in some block one expert is named by exactly 16.
All inputs are finite; a program needn't handle non-finite values.
Results may differ from a plain program's by a relative error of at most 0.014.
The roundings to bfloat16 on the way count: a program that leaves them out, or rounds other values in their place, can miss the bound.
Values may be sent and summed in bfloat16 or wider, within the bound.
A program may use at most 64 MiB of HBM per device.

v0:
```python
import jax
import jax.numpy as jnp
from jax import lax
from jax.sharding import PartitionSpec as P

HEADS = 8
NOPE = 64
ROPE = 32
VDIM = 64
KVLORA = 128
eps = 1e-06
rope_base = 10000.0


def rms_scale(values, gain):
    return values * lax.rsqrt(jnp.mean(values * values, axis=-1, keepdims=True) + eps) * gain


def rotate(values, positions):
    width = values.shape[-1]
    middle = width // 2
    inverse = jnp.power(rope_base, -jnp.arange(0, width, 2).astype(jnp.float32) / width)
    angles = positions.astype(jnp.float32)[:, None] * inverse[None, :]
    angles = jnp.concatenate([angles, angles], axis=-1)
    target = (angles.shape[0],) + (1,) * (values.ndim - 2) + (width,)
    cosine = jnp.cos(angles).reshape(target)
    sine = jnp.sin(angles).reshape(target)
    turned = jnp.concatenate([-values[..., middle:], values[..., :middle]], axis=-1)
    return values * cosine + turned * sine


def route_slots(route_table, expert_count):
    flat_ids = route_table.reshape(-1)
    onehot = (flat_ids[:, None] == jnp.arange(expert_count, dtype=jnp.int32)[None, :]).astype(
        jnp.int32
    )
    before = jnp.cumsum(onehot, axis=0) - onehot
    return jnp.sum(before * onehot, axis=1).reshape(route_table.shape)


def unit_block(arrived, w_gate, w_up, w_down):
    gate_part = jnp.einsum("scd,df->scf", arrived, w_gate[0], preferred_element_type=jnp.float32)
    up_part = jnp.einsum("scd,df->scf", arrived, w_up[0], preferred_element_type=jnp.float32)
    inner = (jax.nn.silu(gate_part) * up_part).astype(jnp.bfloat16)
    block_term = jnp.einsum("scf,fd->scd", inner, w_down[0], preferred_element_type=jnp.float32)
    summed = lax.psum_scatter(
        block_term.astype(jnp.bfloat16), "tp", scatter_dimension=2, tiled=True
    )
    return lax.all_to_all(summed, "ep", split_axis=0, concat_axis=0, tiled=True)


def per_device(
    hidden_in,
    attn_gain,
    w_qdown,
    q_gain,
    w_qnope,
    w_qrope,
    w_kvdown,
    kv_gain,
    w_krope,
    w_ukey,
    w_uvalue,
    w_out,
    cache_latent,
    cache_rope,
    lengths,
    ffn_gain,
    routes,
    route_weights,
    w_gate,
    w_up,
    w_down,
):
    group_rows, width = hidden_in.shape
    own_count = lengths.shape[0]
    tp_rank = lax.axis_index("tp")
    score_scale = (NOPE + ROPE) ** (-0.5)
    own_rows = lax.dynamic_slice_in_dim(hidden_in, tp_rank * own_count, own_count, 0).astype(
        jnp.float32
    )
    normed = rms_scale(own_rows, attn_gain).astype(jnp.bfloat16)
    q_small = rms_scale(
        jnp.dot(normed, w_qdown, preferred_element_type=jnp.float32), q_gain
    ).astype(jnp.bfloat16)
    q_plain = (
        jnp.dot(q_small, w_qnope, preferred_element_type=jnp.float32)
        .astype(jnp.bfloat16)
        .reshape(own_count, HEADS, NOPE)
    )
    q_turned = rotate(
        jnp.dot(q_small, w_qrope, preferred_element_type=jnp.float32).reshape(
            own_count, HEADS, ROPE
        ),
        lengths,
    ).astype(jnp.bfloat16)
    q_latent = jnp.einsum(
        "shn,chn->shc",
        q_plain,
        w_ukey.reshape(KVLORA, HEADS, NOPE),
        preferred_element_type=jnp.float32,
    ).astype(jnp.bfloat16)
    new_latent = rms_scale(
        jnp.dot(normed, w_kvdown, preferred_element_type=jnp.float32), kv_gain
    ).astype(jnp.bfloat16)
    new_rope = rotate(jnp.dot(normed, w_krope, preferred_element_type=jnp.float32), lengths).astype(
        jnp.bfloat16
    )
    past_scores = (
        jnp.einsum("shc,spc->shp", q_latent, cache_latent, preferred_element_type=jnp.float32)
        + jnp.einsum("shr,srp->shp", q_turned, cache_rope, preferred_element_type=jnp.float32)
    ) * score_scale
    in_range = jnp.arange(cache_latent.shape[1])[None, None, :] < lengths[:, None, None]
    past_scores = jnp.where(in_range, past_scores, -1e30)
    fresh_score = (
        jnp.einsum("shc,sc->sh", q_latent, new_latent, preferred_element_type=jnp.float32)
        + jnp.einsum("shr,sr->sh", q_turned, new_rope, preferred_element_type=jnp.float32)
    ) * score_scale
    highest = jnp.maximum(jnp.max(past_scores, axis=-1), fresh_score)
    past_exp = jnp.exp(past_scores - highest[..., None])
    fresh_exp = jnp.exp(fresh_score - highest)
    divisor = jnp.sum(past_exp, axis=-1) + fresh_exp
    past_prob = (past_exp / divisor[..., None]).astype(jnp.bfloat16)
    fresh_prob = (fresh_exp / divisor).astype(jnp.bfloat16)
    latent_mix = (
        jnp.einsum("shp,spc->shc", past_prob, cache_latent, preferred_element_type=jnp.float32)
        + fresh_prob.astype(jnp.float32)[..., None] * new_latent.astype(jnp.float32)[:, None, :]
    ).astype(jnp.bfloat16)
    head_values = (
        jnp.einsum(
            "shc,chv->shv",
            latent_mix,
            w_uvalue.reshape(KVLORA, HEADS, VDIM),
            preferred_element_type=jnp.float32,
        )
        .astype(jnp.bfloat16)
        .reshape(own_count, HEADS * VDIM)
    )
    by_heads = lax.all_to_all(head_values, "tp", split_axis=1, concat_axis=0, tiled=True)
    attended = lax.psum(
        jnp.dot(by_heads, w_out, preferred_element_type=jnp.float32).astype(jnp.bfloat16), "tp"
    ).astype(jnp.float32)
    residual = hidden_in.astype(jnp.float32) + attended
    normed_two = rms_scale(residual, ffn_gain).astype(jnp.bfloat16)
    unit_count = lax.axis_size("ep")
    expert_count = unit_count // 2
    capacity = max(2, 4 * group_rows // expert_count)
    quarter = width // lax.axis_size("tp")
    slots = route_slots(routes, expert_count)
    expert_of_unit = jnp.arange(unit_count, dtype=jnp.int32) // 2
    slot_range = jnp.arange(capacity, dtype=jnp.int32)
    chosen = (routes[None, None, :, :] == expert_of_unit[:, None, None, None]) & (
        slots[None, None, :, :] == slot_range[None, :, None, None]
    )
    chooser = jnp.sum(chosen.astype(jnp.int32), axis=-1).astype(jnp.bfloat16)
    outgoing = jnp.einsum(
        "ucr,rd->ucd", chooser, normed_two, preferred_element_type=jnp.float32
    ).astype(jnp.bfloat16)
    returned = unit_block(
        lax.all_to_all(outgoing, "ep", split_axis=0, concat_axis=0, tiled=True),
        w_gate,
        w_up,
        w_down,
    )
    stacked = returned.reshape(unit_count * capacity, quarter)
    first_row = routes * (2 * capacity) + slots
    first_half = stacked[first_row].astype(jnp.float32)
    second_half = stacked[first_row + capacity].astype(jnp.float32)
    blended = jnp.sum(route_weights[..., None] * (first_half + second_half), axis=1)
    own_columns = lax.dynamic_slice_in_dim(residual, tp_rank * quarter, quarter, 1)
    return (own_columns + blended).astype(jnp.bfloat16)


def solution(mesh):
    placed = (
        P("ep", None),
        P(),
        P(),
        P(),
        P(),
        P(),
        P(),
        P(),
        P(),
        P(),
        P(),
        P("tp", None),
        P(("ep", "tp"), None, None),
        P(("ep", "tp"), None, None),
        P(("ep", "tp")),
        P(),
        P("ep", None),
        P("ep", None),
        P("ep", None, "tp"),
        P("ep", None, "tp"),
        P("ep", "tp", None),
    )
    return jax.shard_map(
        per_device, mesh=mesh, in_specs=placed, out_specs=P("ep", "tp"), check_vma=False
    )
```

profile of v0, /device:TPU:0, one launch (start us, length us, event | category | flops | bytes accessed | tf_op | source)
XLA Modules:
  0.0 95.3 jit_solution(16051706030308229401)
XLA Ops:
  6.5 0.8 convert_element_type.106
  7.3 0.7 iota_compare_fusion.2
  8.0 0.8 fusion.25
  8.9 0.0 copy-start.8
  8.9 1.1 %fusion.49 = f32[4,32]{1,0:T(4,128)S(1)} fusion(bf16[1024,32]{0,1:T(8,128)(2,1)} %param.29, f32[1024]{0:T(1024)} %param.22, f32[4]{0:T(128)S(1)} %add_rsqrt_fusion.3, bf16[16,1024]{1,0:T(8,128)(2,1)S(1)} %copy-done.4, s32[]{:T(128)S(6)} %select_n.25), kind=kOutput, calls=%fused_computation.101 | convolution fusion | flops 278528 | bytes 78852 | tf_op jit(solution)/shard_map/dot_general | solution.py:106
  10.0 1.4 %multiply_reduce_fusion.2 = (f32[4]{0:T(128)S(1)}, f32[4,256]{1,0:T(4,128)S(1)}) fusion(bf16[1024,256]{1,0:T(8,128)(2,1)} %param.23, f32[1024]{0:T(1024)S(1)} %copy-done.8, f32[4]{0:T(128)S(1)} %add_rsqrt_fusion.3, bf16[16,1024]{1,0:T(8,128)(2,1)S(1)} %copy-done.4, s32[]{:T(128)S(6)} %select_n.25), kind=kOutput, calls=%fused_computation.66 | convolution fusion | flops 2115580 | bytes 541204 | tf_op jit(solution)/shard_map/dot_general | solution.py:84
  11.4 0.7 copy-done.16
  12.1 0.2 fusion.48
  12.3 0.1 reshape.175
  12.3 0.1 slice_negate_fusion
  12.4 0.2 convolution_convert_fusion.5
  12.6 0.1 reshape.173
  12.7 0.6 copy-done.5
  13.3 0.1 copy.68
  13.4 0.1 slice_negate_fusion.1
  13.5 0.1 fusion.43
  13.6 0.1 fusion.29
  13.7 0.2 fusion.57
  13.8 0.1 fusion.38
  13.9 0.4 copy-done.14
  14.3 0.3 multiply_reduce_fusion.3
  14.7 0.2 fusion.4
  14.8 0.7 copy-done.11
  15.5 0.1 fusion.55
  15.5 0.1 fusion.33
  15.7 0.5 fusion.56
  16.1 0.2 fusion.17
  16.3 0.7 copy-done.6
  17.1 0.1 copy.71
  17.2 0.3 fusion.3
  17.5 0.2 fusion.5
  17.7 0.1 all_to_all.20
  17.8 0.6 copy.74
  18.4 4.3 %all-to-all-start = ((bf16[4,4,128]{2,0,1:T(4,128)(2,1)}), bf16[4,4,128]{2,0,1:T(4,128)(2,1)S(1)}, u32[]{:S(2)}, u32[]{:S(2)}) async-start(bf16[4,4,128]{2,0,1:T(4,128)(2,1)} %copy.74), calls=%async_computation | async-start | bytes 8192 | tf_op jit(solution)/shard_map/all_to_all | solution.py:139
  22.7 0.1 copy.76
  22.8 0.1 eq.56
  22.9 0.1 fusion.30
  22.9 0.1 reduce_window_sum.11
  23.0 0.2 select_reduce_fusion
  23.2 0.1 eq.60
  23.3 0.1 copy.77
  23.4 0.1 broadcast_compare_fusion
  23.5 3.0 %all-to-all-done = bf16[4,4,128]{2,0,1:T(4,128)(2,1)S(1)} async-done(((bf16[4,4,128]{2,0,1:T(4,128)(2,1)}), bf16[4,4,128]{2,0,1:T(4,128)(2,1)S(1)}, u32[]{:S(2)}, u32[]{:S(2)}) %all-to-all-start) | async-done | bytes 4128 | tf_op jit(solution)/shard_map/all_to_all | solution.py:139
  26.5 0.1 convolution_convert_fusion.2
  26.6 10.3 %psum.7 = bf16[16,1024]{1,0:T(8,128)(2,1)S(1)} all-reduce(bf16[16,1024]{1,0:T(8,128)(2,1)S(1)} %convolution_convert_fusion.2), channel_id=1, replica_groups=mesh['ep'=8,'tp'=4] {'tp'}, use_global_device_ids=true, to_apply=%region_5.6 | all-reduce | flops 16384 | bytes 65536 | tf_op jit(solution)/shard_map/psum | solution.py:140
  36.9 0.1 convert_add_fusion
  37.0 0.3 convolution_convert_fusion
  37.3 15.4 %all_to_all.29 = bf16[8,16,1024]{2,1,0:T(8,128)(2,1)S(1)} all-to-all(bf16[8,16,1024]{2,1,0:T(8,128)(2,1)S(1)} %convolution_convert_fusion), channel_id=1, replica_groups=mesh['ep'=8,'tp'=4] {'ep'}, dimensions={0} | all-to-all | bytes 524288 | tf_op jit(solution)/shard_map/all_to_all | solution.py:160
  52.7 0.4 fusion.9
  53.1 2.6 %convolution_convert_fusion.1 = bf16[8,16,1024]{2,1,0:T(8,128)(2,1)} fusion(bf16[8,16,1024]{2,1,0:T(8,128)(2,1)S(1)} %all_to_all.29, bf16[1,448,1024]{2,1,0:T(8,128)(2,1)S(1)} %copy-done.12, bf16[1,1024,448]{1,2,0:T(8,128)(2,1)} %param.40, f32[8,16,448]{2,1,0:T(8,128)S(1)} %fusion.9), kind=kOutput, calls=%fused_computation.3 | convolution fusion | flops 235356160 | bytes 2588672 | tf_op jit(solution)/shard_map/scf,fd->scd/dot_general | solution.py:45
  55.7 0.0 reduce-scatter.2.cloned.1.call-update
  55.8 0.1 copy.79
  55.8 0.1 reshape.180
  55.9 18.1 %reduce-scatter.2.cloned.1.call-done = bf16[8,16,256]{2,1,0:T(8,128)(2,1)} async-done(((bf16[8,16,1024]{2,1,0:T(8,128)(2,1)}), bf16[8,16,256]{2,1,0:T(8,128)(2,1)}) %reduce-scatter.2.cloned.1.call-update) | async-done | bytes 65552 | tf_op jit(solution)/shard_map/reduce_scatter | solution.py:46
  74.0 5.5 %all-to-all-start.2 = ((bf16[8,16,256]{2,1,0:T(8,128)(2,1)}), bf16[8,16,256]{2,1,0:T(8,128)(2,1)S(1)}, u32[]{:S(2)}, u32[]{:S(2)}) async-start(bf16[8,16,256]{2,1,0:T(8,128)(2,1)} %reduce-scatter.2.cloned.1.call-done), calls=%async_computation.3 | async-start | bytes 131072 | tf_op jit(solution)/shard_map/all_to_all | solution.py:49
  79.5 0.1 copy.80
  79.6 0.1 reshape.188
  79.7 0.6 copy-done.10
  80.3 0.1 copy.75
  80.4 6.0 %all-to-all-done.2 = bf16[8,16,256]{2,1,0:T(8,128)(2,1)S(1)} async-done(((bf16[8,16,256]{2,1,0:T(8,128)(2,1)}), bf16[8,16,256]{2,1,0:T(8,128)(2,1)S(1)}, u32[]{:S(2)}, u32[]{:S(2)}) %all-to-all-start.2) | async-done | bytes 65568 | tf_op jit(solution)/shard_map/all_to_all | solution.py:49
  86.4 0.6 gather_fusion
  87.1 0.6 gather_fusion.1
  87.7 0.1 multiply_reduce_fusion.1
  87.8 0.6 add_convert_fusion
  (44 shorter events, 0.2 us)
Async XLA Ops:
  6.5 9.1 %copy-start = (bf16[4,1024,128]{2,1,0:T(8,128)(2,1)S(1)}, bf16[4,1024,128]{2,1,0:T(8,128)(2,1)}, u32[]{:S(2)}) copy-start(bf16[4,1024,128]{2,1,0:T(8,128)(2,1)} %param.33) | copy-start | bytes 3145732
  6.5 2.3 %copy-start.4 = (bf16[16,1024]{1,0:T(8,128)(2,1)S(1)}, bf16[16,1024]{1,0:T(8,128)(2,1)}, u32[]{:S(2)}) copy-start(bf16[16,1024]{1,0:T(8,128)(2,1)} %param.21) | copy-start | bytes 98308
  8.9 1.1 %copy-start.8 = (f32[1024]{0:T(1024)S(1)}, f32[1024]{0:T(1024)}, u32[]{:S(2)}) copy-start(f32[1024]{0:T(1024)} %param.22) | copy-start | bytes 12292
  10.0 1.5 %copy-start.15 = (bf16[256,256]{1,0:T(8,128)(2,1)S(1)}, bf16[256,256]{1,0:T(8,128)(2,1)}, u32[]{:S(2)}) copy-start(bf16[256,256]{1,0:T(8,128)(2,1)} %param.26) | copy-start | bytes 393220
  10.0 2.5 %copy-start.13 = (bf16[256,512]{1,0:T(8,128)(2,1)S(1)}, bf16[256,512]{1,0:T(8,128)(2,1)}, u32[]{:S(2)}) copy-start(bf16[256,512]{1,0:T(8,128)(2,1)} %param.25) | copy-start | bytes 786436
  11.4 0.7 copy-start.16
  12.3 0.9 copy-start.5
  12.4 1.3 %copy-start.3 = (bf16[4,32,1024]{2,1,0:T(8,128)(2,1)S(1)}, bf16[4,32,1024]{2,1,0:T(8,128)(2,1)}, u32[]{:S(2)}) copy-start(bf16[4,32,1024]{2,1,0:T(8,128)(2,1)} %param.34) | copy-start | bytes 786436
  13.4 1.0 %copy-start.14 = (bf16[1024,128]{1,0:T(8,128)(2,1)S(1)}, bf16[1024,128]{1,0:T(8,128)(2,1)}, u32[]{:S(2)}) copy-start(bf16[1024,128]{1,0:T(8,128)(2,1)} %param.27) | copy-start | bytes 786436
  14.8 0.7 copy-start.11
  16.1 0.9 copy-start.6
  17.2 5.5 %copy-start.7 = (s32[16,2]{0,1:T(2,128)S(1)}, s32[16,2]{0,1:T(2,128)}, u32[]{:S(2)}) copy-start(s32[16,2]{0,1:T(2,128)} %param.37) | copy-start | bytes 388
  17.2 9.3 %copy-start.2 = (bf16[128,1024]{1,0:T(8,128)(2,1)S(1)}, bf16[128,1024]{1,0:T(8,128)(2,1)}, u32[]{:S(2)}) copy-start(bf16[128,1024]{1,0:T(8,128)(2,1)} %param.32) | copy-start | bytes 786436
  17.2 19.8 %copy-start.9 = (f32[1024]{0:T(1024)S(1)}, f32[1024]{0:T(1024)}, u32[]{:S(2)}) copy-start(f32[1024]{0:T(1024)} %param.36) | copy-start | bytes 12292
  17.5 35.2 %copy-start.1 = (bf16[1,1024,448]{1,2,0:T(8,128)(2,1)S(1)}, bf16[1,1024,448]{1,2,0:T(8,128)(2,1)}, u32[]{:S(2)}) copy-start(bf16[1,1024,448]{1,2,0:T(8,128)(2,1)} %param.39) | copy-start | bytes 2752516
  18.4 8.1 %all-to-all-start = ((bf16[4,4,128]{2,0,1:T(4,128)(2,1)}), bf16[4,4,128]{2,0,1:T(4,128)(2,1)S(1)}, u32[]{:S(2)}, u32[]{:S(2)}) async-start(bf16[4,4,128]{2,0,1:T(4,128)(2,1)} %copy.74), calls=%async_computation | async-start | bytes 8192 | tf_op jit(solution)/shard_map/all_to_all | solution.py:139
  22.7 51.3 %reduce-scatter.2.cloned.1.call-start = ((), (), s32[]{:S(2)}) async-start(), calls=%async_computation.4 | async-start | bytes 327680 | tf_op jit(solution)/shard_map/reduce_scatter | solution.py:46
  37.3 15.8 %copy-start.12 = (bf16[1,448,1024]{2,1,0:T(8,128)(2,1)S(1)}, bf16[1,448,1024]{2,1,0:T(8,128)(2,1)}, u32[]{:S(2)}) copy-start(bf16[1,448,1024]{2,1,0:T(8,128)(2,1)} %param.41) | copy-start | bytes 2752516
  74.0 12.4 %all-to-all-start.2 = ((bf16[8,16,256]{2,1,0:T(8,128)(2,1)}), bf16[8,16,256]{2,1,0:T(8,128)(2,1)S(1)}, u32[]{:S(2)}, u32[]{:S(2)}) async-start(bf16[8,16,256]{2,1,0:T(8,128)(2,1)} %reduce-scatter.2.cloned.1.call-done), calls=%async_computation.3 | async-start | bytes 131072 | tf_op jit(solution)/shard_map/all_to_all | solution.py:49
  79.6 0.7 copy-start.10
Sparse Core Ops, SparseCore 0:
  55.9 18.0 reduce-scatter.1
where the time goes:
time: 95.9 us; the launch traced here: 95.3 us
  waiting for transfers between devices  27.1 us (28%)
  blocking collectives  25.6 us (27%)
  between operations  13.6 us (14%)
  starting transfers between devices  9.79 us (10%)
  matrix products  8.07 us (8%)
  local copies, waits for them, and re-layouts  6.79 us (7%)
  other arithmetic  4.28 us (4%)
    reduce_scatter x1, waiting for transfers between devices, unit_block(): lax.psum_scatter(block_term.astype(jnp.bfloat16), 'tp', scatter_dimension...  18.1 us
    all_to_all x1, blocking collectives, per_device(): lax.all_to_all(outgoing, 'ep', split_axis=0, concat_axis=0, tiled=True)  15.4 us
    psum x1, blocking collectives, per_device(): lax.psum(jnp.dot(by_heads, w_out, preferred_element_type=jnp.float32).ast...  10.3 us
    all_to_all x1, waiting for transfers between devices, unit_block(): return lax.all_to_all(summed, 'ep', split_axis=0, concat_axis=0, tiled=True)  6.04 us
    all_to_all x1, starting transfers between devices, unit_block(): return lax.all_to_all(summed, 'ep', split_axis=0, concat_axis=0, tiled=True)  5.52 us
    all_to_all x1, starting transfers between devices, per_device(): lax.all_to_all(head_values, 'tp', split_axis=1, concat_axis=0, tiled=True)  4.26 us
    unnamed x38, local copies, waits for them, and re-layouts  4.04 us
    all_to_all x1, waiting for transfers between devices, per_device(): lax.all_to_all(head_values, 'tp', split_axis=1, concat_axis=0, tiled=True)  2.99 us
  transfers between devices with their start and end apart: 3, of which 3 were waited for; matrix products, arithmetic and copies ran while one was open for 1% of the time, Pallas kernels for 0%

commit v1 on v0

--- a/solution.py
+++ b/solution.py
@@ -137,8 +137,11 @@
         .reshape(own_count, HEADS * VDIM)
     )
     by_heads = lax.all_to_all(head_values, "tp", split_axis=1, concat_axis=0, tiled=True)
-    attended = lax.psum(
-        jnp.dot(by_heads, w_out, preferred_element_type=jnp.float32).astype(jnp.bfloat16), "tp"
+    attended = jnp.sum(
+        lax.all_gather(
+            jnp.dot(by_heads, w_out, preferred_element_type=jnp.float32).astype(jnp.bfloat16), "tp"
+        ),
+        axis=0,
     ).astype(jnp.float32)
     residual = hidden_in.astype(jnp.float32) + attended
     normed_two = rms_scale(residual, ffn_gain).astype(jnp.bfloat16)

time: 95.9 us -> 91.3 us (0.952)
  blocking collectives: 25.6 us -> 21 us
    psum x1 -> x0, blocking collectives: 10.3 us -> none  [per_device(): lax.psum(jnp.dot(by_heads, w_out, preferred_element_type=jnp.float32).ast...]
    all_gather x0 -> x1, blocking collectives: none -> 5.41 us  [per_device(): lax.all_gather(jnp.dot(by_heads, w_out, preferred_element_type=jnp.float3...]
where the time goes in v1:
time: 91.3 us; the launch traced here: 90.7 us
  waiting for transfers between devices  27.1 us (30%)
  blocking collectives  21 us (23%)
  between operations  13.6 us (15%)
  starting transfers between devices  9.79 us (11%)
  matrix products  8.07 us (9%)
  local copies, waits for them, and re-layouts  6.78 us (7%)
  other arithmetic  4.3 us (5%)
    reduce_scatter x1, waiting for transfers between devices, unit_block(): lax.psum_scatter(block_term.astype(jnp.bfloat16), 'tp', scatter_dimension...  18.1 us
    all_to_all x1, blocking collectives, per_device(): lax.all_to_all(outgoing, 'ep', split_axis=0, concat_axis=0, tiled=True)  15.6 us
    all_to_all x1, waiting for transfers between devices, unit_block(): return lax.all_to_all(summed, 'ep', split_axis=0, concat_axis=0, tiled=True)  6.04 us
    all_to_all x1, starting transfers between devices, unit_block(): return lax.all_to_all(summed, 'ep', split_axis=0, concat_axis=0, tiled=True)  5.52 us
    all_gather x1, blocking collectives, per_device(): lax.all_gather(jnp.dot(by_heads, w_out, preferred_element_type=jnp.float3...  5.41 us
    all_to_all x1, starting transfers between devices, per_device(): lax.all_to_all(head_values, 'tp', split_axis=1, concat_axis=0, tiled=True)  4.26 us
    unnamed x38, local copies, waits for them, and re-layouts  4.03 us
    all_to_all x1, waiting for transfers between devices, per_device(): lax.all_to_all(head_values, 'tp', split_axis=1, concat_axis=0, tiled=True)  2.99 us
  transfers between devices with their start and end apart: 3, of which 3 were waited for; matrix products, arithmetic and copies ran while one was open for 1% of the time, Pallas kernels for 0%

profile of v1, /device:TPU:0, one launch (start us, length us, event | category | flops | bytes accessed | tf_op | source)
XLA Modules:
  0.0 90.7 jit_solution(11457408909504775691)
XLA Ops:
  6.5 0.8 convert_element_type.108
  7.3 0.7 iota_compare_fusion.2
  8.0 0.8 fusion.25
  8.9 0.0 copy-start.8
  8.9 1.1 %fusion.49 = f32[4,32]{1,0:T(4,128)S(1)} fusion(bf16[1024,32]{0,1:T(8,128)(2,1)} %param.29, f32[1024]{0:T(1024)} %param.22, f32[4]{0:T(128)S(1)} %add_rsqrt_fusion.3, bf16[16,1024]{1,0:T(8,128)(2,1)S(1)} %copy-done.4, s32[]{:T(128)S(6)} %select_n.25), kind=kOutput, calls=%fused_computation.101 | convolution fusion | flops 278528 | bytes 78852 | tf_op jit(solution)/shard_map/dot_general | solution.py:106
  10.0 1.4 %multiply_reduce_fusion.2 = (f32[4]{0:T(128)S(1)}, f32[4,256]{1,0:T(4,128)S(1)}) fusion(bf16[1024,256]{1,0:T(8,128)(2,1)} %param.23, f32[1024]{0:T(1024)S(1)} %copy-done.8, f32[4]{0:T(128)S(1)} %add_rsqrt_fusion.3, bf16[16,1024]{1,0:T(8,128)(2,1)S(1)} %copy-done.4, s32[]{:T(128)S(6)} %select_n.25), kind=kOutput, calls=%fused_computation.66 | convolution fusion | flops 2115580 | bytes 541204 | tf_op jit(solution)/shard_map/dot_general | solution.py:84
  11.4 0.7 copy-done.16
  12.1 0.2 fusion.48
  12.3 0.1 reshape.175
  12.3 0.1 slice_negate_fusion
  12.4 0.2 convolution_convert_fusion.5
  12.6 0.1 reshape.173
  12.7 0.6 copy-done.5
  13.3 0.1 copy.68
  13.4 0.1 slice_negate_fusion.1
  13.5 0.1 fusion.43
  13.6 0.1 fusion.29
  13.7 0.2 fusion.57
  13.8 0.1 fusion.38
  13.9 0.4 copy-done.14
  14.3 0.3 multiply_reduce_fusion.3
  14.7 0.2 fusion.4
  14.8 0.7 copy-done.11
  15.5 0.1 fusion.55
  15.5 0.1 fusion.33
  15.7 0.5 fusion.56
  16.1 0.2 fusion.17
  16.3 0.7 copy-done.6
  17.1 0.1 copy.71
  17.2 0.3 fusion.3
  17.5 0.2 fusion.5
  17.7 0.1 all_to_all.20
  17.8 0.6 copy.74
  18.4 4.3 %all-to-all-start = ((bf16[4,4,128]{2,0,1:T(4,128)(2,1)}), bf16[4,4,128]{2,0,1:T(4,128)(2,1)S(1)}, u32[]{:S(2)}, u32[]{:S(2)}) async-start(bf16[4,4,128]{2,0,1:T(4,128)(2,1)} %copy.74), calls=%async_computation | async-start | bytes 8192 | tf_op jit(solution)/shard_map/all_to_all | solution.py:139
  22.7 0.1 copy.76
  22.7 0.1 eq.56
  22.8 0.1 fusion.30
  22.9 0.1 reduce_window_sum.11
  23.0 0.2 select_reduce_fusion
  23.2 0.1 eq.60
  23.2 0.1 copy.77
  23.3 0.1 broadcast_compare_fusion
  23.5 3.0 %all-to-all-done = bf16[4,4,128]{2,0,1:T(4,128)(2,1)S(1)} async-done(((bf16[4,4,128]{2,0,1:T(4,128)(2,1)}), bf16[4,4,128]{2,0,1:T(4,128)(2,1)S(1)}, u32[]{:S(2)}, u32[]{:S(2)}) %all-to-all-start) | async-done | bytes 4128 | tf_op jit(solution)/shard_map/all_to_all | solution.py:139
  26.4 0.1 convolution_convert_fusion.2
  26.6 5.4 %all-gather = bf16[64,1024]{1,0:T(8,128)(2,1)S(1)} all-gather(bf16[16,1024]{1,0:T(8,128)(2,1)S(1)} %convolution_convert_fusion.2), channel_id=2, replica_groups=mesh['ep'=8,'tp'=4] {'tp'}, dimensions={0}, use_global_device_ids=true | all-gather | bytes 163840 | tf_op jit(solution)/shard_map/all_gather | solution.py:141
  32.0 0.1 convert_add_fusion
  32.2 0.3 convolution_convert_fusion
  32.5 15.6 %all_to_all.29 = bf16[8,16,1024]{2,1,0:T(8,128)(2,1)S(1)} all-to-all(bf16[8,16,1024]{2,1,0:T(8,128)(2,1)S(1)} %convolution_convert_fusion), channel_id=1, replica_groups=mesh['ep'=8,'tp'=4] {'ep'}, dimensions={0} | all-to-all | bytes 524288 | tf_op jit(solution)/shard_map/all_to_all | solution.py:163
  48.1 0.4 fusion.9
  48.5 2.6 %convolution_convert_fusion.1 = bf16[8,16,1024]{2,1,0:T(8,128)(2,1)} fusion(bf16[8,16,1024]{2,1,0:T(8,128)(2,1)S(1)} %all_to_all.29, bf16[1,448,1024]{2,1,0:T(8,128)(2,1)S(1)} %copy-done.12, bf16[1,1024,448]{1,2,0:T(8,128)(2,1)} %param.40, f32[8,16,448]{2,1,0:T(8,128)S(1)} %fusion.9), kind=kOutput, calls=%fused_computation.3 | convolution fusion | flops 235356160 | bytes 2588672 | tf_op jit(solution)/shard_map/scf,fd->scd/dot_general | solution.py:45
  51.1 0.0 reduce-scatter.2.cloned.1.call-update
  51.1 0.1 copy.79
  51.2 0.1 reshape.180
  51.3 18.1 %reduce-scatter.2.cloned.1.call-done = bf16[8,16,256]{2,1,0:T(8,128)(2,1)} async-done(((bf16[8,16,1024]{2,1,0:T(8,128)(2,1)}), bf16[8,16,256]{2,1,0:T(8,128)(2,1)}) %reduce-scatter.2.cloned.1.call-update) | async-done | bytes 65552 | tf_op jit(solution)/shard_map/reduce_scatter | solution.py:46
  69.4 5.5 %all-to-all-start.2 = ((bf16[8,16,256]{2,1,0:T(8,128)(2,1)}), bf16[8,16,256]{2,1,0:T(8,128)(2,1)S(1)}, u32[]{:S(2)}, u32[]{:S(2)}) async-start(bf16[8,16,256]{2,1,0:T(8,128)(2,1)} %reduce-scatter.2.cloned.1.call-done), calls=%async_computation.3 | async-start | bytes 131072 | tf_op jit(solution)/shard_map/all_to_all | solution.py:49
  74.9 0.1 copy.80
  75.0 0.1 reshape.188
  75.1 0.6 copy-done.10
  75.7 0.1 copy.75
  75.8 6.0 %all-to-all-done.2 = bf16[8,16,256]{2,1,0:T(8,128)(2,1)S(1)} async-done(((bf16[8,16,256]{2,1,0:T(8,128)(2,1)}), bf16[8,16,256]{2,1,0:T(8,128)(2,1)S(1)}, u32[]{:S(2)}, u32[]{:S(2)}) %all-to-all-start.2) | async-done | bytes 65568 | tf_op jit(solution)/shard_map/all_to_all | solution.py:49
  81.8 0.6 gather_fusion
  82.4 0.6 gather_fusion.1
  83.1 0.1 multiply_reduce_fusion.1
  83.2 0.6 add_convert_fusion
  (45 shorter events, 0.2 us)
Async XLA Ops:
  6.5 9.1 %copy-start = (bf16[4,1024,128]{2,1,0:T(8,128)(2,1)S(1)}, bf16[4,1024,128]{2,1,0:T(8,128)(2,1)}, u32[]{:S(2)}) copy-start(bf16[4,1024,128]{2,1,0:T(8,128)(2,1)} %param.33) | copy-start | bytes 3145732
  6.5 2.3 %copy-start.4 = (bf16[16,1024]{1,0:T(8,128)(2,1)S(1)}, bf16[16,1024]{1,0:T(8,128)(2,1)}, u32[]{:S(2)}) copy-start(bf16[16,1024]{1,0:T(8,128)(2,1)} %param.21) | copy-start | bytes 98308
  8.9 1.1 %copy-start.8 = (f32[1024]{0:T(1024)S(1)}, f32[1024]{0:T(1024)}, u32[]{:S(2)}) copy-start(f32[1024]{0:T(1024)} %param.22) | copy-start | bytes 12292
  10.0 1.5 %copy-start.15 = (bf16[256,256]{1,0:T(8,128)(2,1)S(1)}, bf16[256,256]{1,0:T(8,128)(2,1)}, u32[]{:S(2)}) copy-start(bf16[256,256]{1,0:T(8,128)(2,1)} %param.26) | copy-start | bytes 393220
  10.0 2.5 %copy-start.13 = (bf16[256,512]{1,0:T(8,128)(2,1)S(1)}, bf16[256,512]{1,0:T(8,128)(2,1)}, u32[]{:S(2)}) copy-start(bf16[256,512]{1,0:T(8,128)(2,1)} %param.25) | copy-start | bytes 786436
  11.4 0.7 copy-start.16
  12.3 0.9 %copy-start.5 = (bf16[128,512]{1,0:T(8,128)(2,1)S(1)}, bf16[128,512]{1,0:T(8,128)(2,1)}, u32[]{:S(2)}) copy-start(bf16[128,512]{1,0:T(8,128)(2,1)} %param.30) | copy-start | bytes 393220
  12.4 1.3 %copy-start.3 = (bf16[4,32,1024]{2,1,0:T(8,128)(2,1)S(1)}, bf16[4,32,1024]{2,1,0:T(8,128)(2,1)}, u32[]{:S(2)}) copy-start(bf16[4,32,1024]{2,1,0:T(8,128)(2,1)} %param.34) | copy-start | bytes 786436
  13.4 1.0 %copy-start.14 = (bf16[1024,128]{1,0:T(8,128)(2,1)S(1)}, bf16[1024,128]{1,0:T(8,128)(2,1)}, u32[]{:S(2)}) copy-start(bf16[1024,128]{1,0:T(8,128)(2,1)} %param.27) | copy-start | bytes 786436
  14.8 0.7 copy-start.11
  16.1 0.9 %copy-start.6 = (bf16[128,512]{1,0:T(8,128)(2,1)S(1)}, bf16[128,512]{1,0:T(8,128)(2,1)}, u32[]{:S(2)}) copy-start(bf16[128,512]{1,0:T(8,128)(2,1)} %param.31) | copy-start | bytes 393220
  17.2 5.5 %copy-start.7 = (s32[16,2]{0,1:T(2,128)S(1)}, s32[16,2]{0,1:T(2,128)}, u32[]{:S(2)}) copy-start(s32[16,2]{0,1:T(2,128)} %param.37) | copy-start | bytes 388
  17.5 9.0 %copy-start.2 = (bf16[128,1024]{1,0:T(8,128)(2,1)S(1)}, bf16[128,1024]{1,0:T(8,128)(2,1)}, u32[]{:S(2)}) copy-start(bf16[128,1024]{1,0:T(8,128)(2,1)} %param.32) | copy-start | bytes 786436
  17.7 14.5 %copy-start.9 = (f32[1024]{0:T(1024)S(1)}, f32[1024]{0:T(1024)}, u32[]{:S(2)}) copy-start(f32[1024]{0:T(1024)} %param.36) | copy-start | bytes 12292
  18.4 8.1 %all-to-all-start = ((bf16[4,4,128]{2,0,1:T(4,128)(2,1)}), bf16[4,4,128]{2,0,1:T(4,128)(2,1)S(1)}, u32[]{:S(2)}, u32[]{:S(2)}) async-start(bf16[4,4,128]{2,0,1:T(4,128)(2,1)} %copy.74), calls=%async_computation | async-start | bytes 8192 | tf_op jit(solution)/shard_map/all_to_all | solution.py:139
  22.7 46.7 %reduce-scatter.2.cloned.1.call-start = ((), (), s32[]{:S(2)}) async-start(), calls=%async_computation.4 | async-start | bytes 327680 | tf_op jit(solution)/shard_map/reduce_scatter | solution.py:46
  22.9 25.1 %copy-start.1 = (bf16[1,1024,448]{1,2,0:T(8,128)(2,1)S(1)}, bf16[1,1024,448]{1,2,0:T(8,128)(2,1)}, u32[]{:S(2)}) copy-start(bf16[1,1024,448]{1,2,0:T(8,128)(2,1)} %param.39) | copy-start | bytes 2752516
  32.5 16.0 %copy-start.12 = (bf16[1,448,1024]{2,1,0:T(8,128)(2,1)S(1)}, bf16[1,448,1024]{2,1,0:T(8,128)(2,1)}, u32[]{:S(2)}) copy-start(bf16[1,448,1024]{2,1,0:T(8,128)(2,1)} %param.41) | copy-start | bytes 2752516
  69.4 12.4 %all-to-all-start.2 = ((bf16[8,16,256]{2,1,0:T(8,128)(2,1)}), bf16[8,16,256]{2,1,0:T(8,128)(2,1)S(1)}, u32[]{:S(2)}, u32[]{:S(2)}) async-start(bf16[8,16,256]{2,1,0:T(8,128)(2,1)} %reduce-scatter.2.cloned.1.call-done), calls=%async_computation.3 | async-start | bytes 131072 | tf_op jit(solution)/shard_map/all_to_all | solution.py:49
  75.0 0.7 copy-start.10
Sparse Core Ops, SparseCore 0:
  51.2 18.0 reduce-scatter.1
